TPU v7x, 32 devices: a whole 2x2x4 slice. The times are simulated.
32 devices in a mesh: ep: 8 (over z, x), tp: 4 (over y, core).
Axes of the slice: x: 2, y: 2, z: 4, core: 2. Of those that a mesh axis runs over, the one named last changes fastest.
Arguments:
- queries: bfloat16 [1024, 4096], P('ep', 'tp'), may hold values from -112 to 112
- key_rows: bfloat16 [1024, 4096], P('ep', 'tp'), may hold values from -8.1 to 8.1
- values: bfloat16 [1024, 4096], P('ep', 'tp'), may hold values from -6 to 6
- lambdas: float32 [16], P('tp'), may hold values from 0.3 to 0.8
- head_gain: float32 [256], replicated, may hold values from 0.1 to 1.9
- tokens: bfloat16 [512, 4096], P('ep'), may hold values from -6 to 6
- moe_gain: float32 [4096], replicated, may hold values from 0.1 to 1.9
- routes: int32 [512, 2], P('ep'), may hold values from 0 to 7, all different within a row; in each aligned block of 64 rows (0 to 63, 64 to 127, ...) at most 32 rows name the same one
- route_scores: float32 [512, 2], P('ep'), may hold values from -6 to 6
- w_gate: bfloat16 [8, 4096, 2048], P('ep', None, 'tp'), may hold values from -0.09375 to 0.09375
- w_up: bfloat16 [8, 4096, 2048], P('ep', None, 'tp'), may hold values from -0.09375 to 0.09375
- w_down: bfloat16 [8, 2048, 4096], P('ep', 'tp'), may hold values from -0.125 to 0.125
Outputs:
- attended: bfloat16 [1024, 4096], P('ep', 'tp')
- expert_out: bfloat16 [512, 4096], P('ep', 'tp')
Inputs may be any that keep to these rules, and one draw needn't show every extreme that they name: `routes`: each row names 2 different experts. Among the rows of one index of ep at most 32 name the same expert, and some index reaches 32 in every draw.
All inputs are finite; a program needn't handle non-finite values.
Results may differ from a plain program's by a relative error of at most 0.018.
Values may be sent and summed in bfloat16 or wider, within the bound.
A program may use at most 64 MiB of HBM per device.

v0:
```python
import jax
import jax.numpy as jnp
from jax import lax
from jax.sharding import PartitionSpec as P

QKD = 128
VD = 256
TOP = 2


neg_big = -1e30
head_eps = 1e-05
moe_eps = 1e-06
head_scale = 0.8


def slot_table(routes, experts, capacity):
    flat_routes = routes.reshape(-1)
    onehot = (flat_routes[:, None] == jnp.arange(experts, dtype=jnp.int32)[None, :]).astype(
        jnp.int32
    )
    before = jnp.cumsum(onehot, axis=0) - onehot
    position = jnp.sum(before * onehot, axis=1)
    return (flat_routes * capacity + position).reshape(routes.shape)


def fold_block(state, query_group, query_pos, key_heads, value_heads, key_pos):
    maxima, denominators, accumulated = state
    scores = jnp.einsum(
        "qhmd,khmd->hmqk", query_group, key_heads, preferred_element_type=jnp.float32
    ) * QKD ** (-0.5)
    visible = key_pos[None, :] <= query_pos[:, None]
    scores = jnp.where(visible, scores, neg_big)
    new_max = jnp.maximum(maxima, jnp.max(scores, axis=-1))
    weights = jnp.where(visible, jnp.exp(scores - new_max[..., None]), 0.0)
    accumulated = jnp.einsum(
        "hmqk,khd->hmqd", weights, value_heads, precision=lax.Precision.HIGHEST
    )
    denominators = jnp.sum(weights, axis=-1)
    return (new_max, denominators, accumulated)


def local(
    queries,
    key_rows,
    values,
    lambdas,
    head_gain,
    tokens,
    moe_gain,
    routes,
    route_scores,
    w_gate,
    w_up,
    w_down,
):
    rows_a = queries.shape[0]
    half_rows = rows_a // 2
    head_local = lambdas.shape[0]
    ep_count = lax.axis_size("ep")
    ep_index = lax.axis_index("ep")
    early_queries = queries[:half_rows]
    later_queries = queries[half_rows:]
    early_pos = ep_index * rows_a + jnp.arange(half_rows, dtype=jnp.int32)
    later_pos = ep_index * rows_a + half_rows + jnp.arange(half_rows, dtype=jnp.int32)
    query_groups = (
        early_queries.reshape(half_rows, head_local, 2, QKD),
        later_queries.reshape(half_rows, head_local, 2, QKD),
    )
    position_groups = (early_pos, later_pos)
    start_state = (
        jnp.full((head_local, 2, half_rows), neg_big, jnp.float32),
        jnp.zeros((head_local, 2, half_rows), jnp.float32),
        jnp.zeros((head_local, 2, half_rows, VD), jnp.float32),
    )
    totals = (start_state, start_state)
    row_start = jnp.int32(0)
    key_block = lax.all_gather(key_rows, "ep", axis=0, tiled=True)
    value_block = lax.all_gather(values, "ep", axis=0, tiled=True)
    key_count = key_block.shape[0]
    key_heads = key_block.reshape(key_count, head_local, 2, QKD)
    value_heads = value_block.reshape(key_count, head_local, VD).astype(jnp.float32)
    key_pos = jnp.arange(key_count, dtype=jnp.int32)
    updated = []
    for attend_group_index in range(2):
        state = totals[attend_group_index]
        query_group = query_groups[attend_group_index]
        query_pos = position_groups[attend_group_index]
        state = lax.cond(
            row_start <= query_pos[-1],
            lambda held: fold_block(held, query_group, query_pos, key_heads, value_heads, key_pos),
            lambda held: held,
            state,
        )
        updated.append(state)
    folded = (updated[0], updated[1])
    attended_groups = []
    for group_index in range(2):
        maxima, denominators, accumulated = folded[group_index]
        mixed_out = (
            accumulated[:, 0] / denominators[:, 0, :, None]
            - lambdas[:, None, None] * accumulated[:, 1] / denominators[:, 1, :, None]
        )
        scaled = mixed_out * lax.rsqrt(
            jnp.mean(mixed_out * mixed_out, axis=-1, keepdims=True) + head_eps
        )
        scaled = scaled * head_gain * head_scale
        attended_groups.append(
            scaled.transpose(1, 0, 2).reshape(half_rows, head_local * VD).astype(jnp.bfloat16)
        )
    later_out = attended_groups[1]
    attended = jnp.concatenate([attended_groups[0], later_out], axis=0)
    rows_b = tokens.shape[0]
    capacity = 2 * TOP * rows_b // ep_count
    token_f32 = tokens.astype(jnp.float32)
    normed = (
        token_f32
        * lax.rsqrt(jnp.mean(token_f32 * token_f32, axis=-1, keepdims=True) + moe_eps)
        * moe_gain
    ).astype(jnp.bfloat16)
    gate_weights = jax.nn.softmax(route_scores, axis=-1)
    slot_of = slot_table(routes, ep_count, capacity)
    row_ids = jnp.broadcast_to(jnp.arange(rows_b, dtype=jnp.int32)[:, None], slot_of.shape)
    row_of_slot = (
        jnp.zeros((ep_count * capacity,), jnp.int32)
        .at[slot_of.reshape(-1)]
        .set(row_ids.reshape(-1))
    )
    gate_local = w_gate[0]
    up_local = w_up[0]
    down_local = w_down[0]
    outgoing = normed[row_of_slot]
    arrived = lax.all_to_all(outgoing, "ep", split_axis=0, concat_axis=0, tiled=True)
    gate_act = jnp.dot(arrived, gate_local, preferred_element_type=jnp.float32)
    up_act = jnp.dot(arrived, up_local, preferred_element_type=jnp.float32)
    hidden = (jax.nn.silu(gate_act) * up_act).astype(jnp.bfloat16)
    summed = lax.psum_scatter(
        lax.dot_general(
            down_local, hidden, (((0,), (1,)), ((), ())), preferred_element_type=jnp.float32
        ).astype(jnp.bfloat16),
        "tp",
        scatter_dimension=0,
        tiled=True,
    )
    returned = lax.all_to_all(summed, "ep", split_axis=1, concat_axis=1, tiled=True)
    slot_ids = jnp.arange(ep_count * capacity, dtype=jnp.int32)
    combined = jnp.zeros((rows_b, returned.shape[0]), jnp.float32)
    for choice_index in range(TOP):
        picker = (slot_of[:, choice_index, None] == slot_ids[None, :]).astype(jnp.bfloat16)
        picked = lax.dot_general(
            picker, returned, (((1,), (1,)), ((), ())), preferred_element_type=jnp.float32
        )
        combined = combined + gate_weights[:, choice_index, None] * picked
    expert_out = combined.astype(jnp.bfloat16)
    return (attended, expert_out)


def solution(mesh):
    return jax.shard_map(
        local,
        mesh=mesh,
        in_specs=(
            P("ep", "tp"),
            P("ep", "tp"),
            P("ep", "tp"),
            P("tp"),
            P(),
            P("ep", None),
            P(),
            P("ep", None),
            P("ep", None),
            P("ep", None, "tp"),
            P("ep", None, "tp"),
            P("ep", "tp", None),
        ),
        out_specs=(P("ep", "tp"), P("ep", "tp")),
        check_vma=False,
    )
```

profile of v0, /device:TPU:0, one launch (start us, length us, event | category | flops | bytes accessed | tf_op | source)
XLA Modules:
  0.0 190.7 jit_solution(13893074613434656306)
XLA Ops:
  8.0 0.0 copy-start.2
  8.0 0.0 all-gather.5.cloned.1.call-start
  8.1 1.9 copy.24
  9.9 0.0 all-gather.5.cloned.1.call-update
  9.9 0.8 copy.34
  10.7 0.1 eq.45
  10.8 0.1 fusion.62
  10.9 0.2 reduce_window_sum.11
  11.1 0.2 select_reduce_fusion
  11.3 0.1 reduce_sum.71
  11.5 0.1 mul.157
  11.6 0.1 reshape.129
  11.8 1.0 scatter_custom_fusion
  12.8 1.2 fusion.42
  14.0 0.0 copy-done.2
  14.0 0.9 fusion.44
  15.0 3.2 %gather_fusion = bf16[256,4096]{1,0:T(8,128)(2,1)} fusion(bf16[64,4096]{1,0:T(8,128)(2,1)S(1)} %fusion.44, s32[1024]{0:T(1024)S(1)} %pad_clamp_fusion), kind=kCustom, calls=%fused_computation | custom fusion | bytes 4195328 | tf_op jit(solution)/shard_map/gather | solution.py:132
  18.2 0.0 copy-start.3
  18.2 7.4 %all-to-all-start = ((bf16[8,32,4096]{2,1,0:T(8,128)(2,1)}), bf16[8,32,4096]{2,1,0:T(8,128)(2,1)S(1)}, u32[]{:S(2)}, u32[]{:S(2)}) async-start(bf16[8,32,4096]{2,1,0:T(8,128)(2,1)} %bitcast.20), calls=%async_computation | async-start | bytes 4194304 | tf_op jit(solution)/shard_map/all_to_all | solution.py:133
  25.6 0.0 all-gather.3.cloned.1.call-start
  25.6 0.0 copy-done.3
  25.6 0.8 copy.23
  26.5 0.0 all-gather.3.cloned.1.call-update
  26.5 0.0 reduce-scatter.2.cloned.1.call-start
  26.5 69.8 %all-to-all-done = bf16[8,32,4096]{2,1,0:T(8,128)(2,1)S(1)} async-done(((bf16[8,32,4096]{2,1,0:T(8,128)(2,1)}), bf16[8,32,4096]{2,1,0:T(8,128)(2,1)S(1)}, u32[]{:S(2)}, u32[]{:S(2)}) %all-to-all-start) | async-done | bytes 2097184 | tf_op jit(solution)/shard_map/all_to_all | solution.py:133
  96.3 3.5 %fusion.32 = f32[256,512]{1,0:T(8,128)S(1)} fusion(bf16[256,4096]{1,0:T(8,128)(2,1)S(1)} %bitcast.99, bf16[1,4096,512]{2,1,0:T(8,128)(2,1)} %param.25), kind=kOutput, calls=%fused_computation.43 | convolution fusion | flops 1073741824 | bytes 6815744 | tf_op jit(solution)/shard_map/dot_general | solution.py:134
  99.8 7.4 %fusion.28 = bf16[4096,256]{0,1:T(8,128)(2,1)} fusion(bf16[1,512,4096]{2,1,0:T(8,128)(2,1)} %param.27, bf16[256,4096]{1,0:T(8,128)(2,1)S(1)} %bitcast.100, bf16[1,4096,512]{2,1,0:T(8,128)(2,1)} %param.26, f32[256,512]{1,0:T(8,128)S(1)} %fusion.32), kind=kOutput, calls=%fused_computation.39 | convolution fusion | flops 2149318656 | bytes 13107200 | tf_op jit(solution)/shard_map/dot_general | solution.py:138
  107.2 0.0 copy-start.5
  107.2 0.0 reduce-scatter.2.cloned.1.call-update
  107.2 0.6 slice.55
  108.5 0.6 slice.50
  109.7 0.0 copy-done.5
  109.8 0.2 slice_reduce_fusion
  110.0 0.0 all-gather.5.cloned.1.call-done
  110.0 0.0 copy-start.4
  110.0 4.1 %convert.3 = f32[1024,4,256]{0,2,1:T(8,128)} convert(bf16[1024,4,256]{0,2,1:T(8,128)(2,1)} %bitcast.98) | non-fusion elementwise | flops 1048576 | bytes 6291456 | tf_op jit(solution)/shard_map/convert_element_type | solution.py:82
  114.1 33.2 %all-gather.3.cloned.1.call-done = bf16[1024,1024]{0,1:T(8,128)(2,1)} async-done(((bf16[128,1024]{0,1:T(8,128)(2,1)}), bf16[1024,1024]{0,1:T(8,128)(2,1)}) %all-gather.3.cloned.1.call-update) | async-done | bytes 2097168 | tf_op jit(solution)/shard_map/all_gather | solution.py:78
  147.3 0.0 copy-done.4
  147.3 8.6 %conditional.3 = (f32[4,2,64]{2,1,0:T(2,128)S(1)}, f32[4,2,64,256]{3,2,1,0:T(8,128)S(1)}) conditional(s32[]{:T(128)} %bitcast.10, () %tuple.26, (s32[1024]{0:T(1024)S(1)}, s32[64]{0:T(128)S(1)}, bf16[128,1024]{1,0:T(8,128)(2,1)S(1)}, bf16[1024,4,2,128]{0,3,2,1:T(8,128)(2,1)}, f32[1024,4,256]{0,2,1:T(8,128)}) %tuple.56), branch_computations={%region_5.6_spmd, %region_6.9_spmd} | conditional | flops 1751186944 | bytes 30818604 | solution.py:89
  147.3 0.1 broadcast_compare_fusion.1
  147.4 0.1 reshape.109
  147.5 0.0 copy-start
  147.5 2.4 %fusion.16 = (f32[4,2,64]{2,1,0:T(2,128)S(1)}, f32[4,2,64,1024]{3,2,1,0:T(8,128)S(1)}) fusion(pred[64,1024]{1,0:T(8,128)(4,1)S(1)} %broadcast_compare_fusion.1, bf16[1024,4,2,128]{0,3,2,1:T(8,128)(2,1)} %get-tuple-element.52, bf16[64,4,2,128]{3,2,1,0:T(2,128)(2,1)S(1)} %reshape.109), kind=kOutput, calls=%fused_computation.24 | convolution fusion | flops 135790080 | bytes 4392960 | tf_op jit(solution)/shard_map/cond/branch_1_fun/qhmd,khmd->hmqk/dot_general | solution.py:29
  150.0 0.4 copy-done
  150.3 4.8 %fusion.14 = f32[4,2,64,256]{3,2,1,0:T(8,128)S(1)} fusion(f32[1024,4,256]{0,2,1:T(8,128)S(1)} %copy-done, f32[4,2,64,1024]{3,2,1,0:T(8,128)S(1)} %get-tuple-element.63, f32[4,2,64]{2,1,0:T(2,128)S(1)} %broadcast_maximum_fusion.1, pred[64,1024]{1,0:T(8,128)(4,1)S(1)} %broadcast_compare_fusion.1), kind=kOutput, calls=%fused_computation.20 | convolution fusion | flops 1612709888 | bytes 6883328 | tf_op jit(solution)/shard_map/cond/branch_1_fun/hmqk,khd->hmqd/dot_general | solution.py:36
  155.2 0.7 fusion.17
  155.9 8.8 %conditional.2 = (f32[4,2,64]{2,1,0:T(2,128)S(1)}, f32[4,2,64,256]{3,2,1,0:T(8,128)S(1)}) conditional(s32[]{:T(128)} %bitcast.2, () %tuple.24, (s32[1024]{0:T(1024)S(1)}, s32[64]{0:T(128)S(1)}, bf16[128,1024]{1,0:T(8,128)(2,1)S(1)}, bf16[1024,4,2,128]{0,3,2,1:T(8,128)(2,1)}, f32[1024,4,256]{0,2,1:T(8,128)}) %tuple.57), branch_computations={%region_0.0_spmd, %region_1.4_spmd} | conditional | flops 1751186944 | bytes 30818604 | solution.py:89
  156.1 0.1 broadcast_compare_fusion
  156.2 0.1 reshape.108
  156.3 0.0 copy-start.1
  156.3 2.4 %fusion.2 = (f32[4,2,64]{2,1,0:T(2,128)S(1)}, f32[4,2,64,1024]{3,2,1,0:T(8,128)S(1)}) fusion(pred[64,1024]{1,0:T(8,128)(4,1)S(1)} %broadcast_compare_fusion, bf16[1024,4,2,128]{0,3,2,1:T(8,128)(2,1)} %get-tuple-element.47, bf16[64,4,2,128]{3,2,1,0:T(2,128)(2,1)S(1)} %reshape.108), kind=kOutput, calls=%fused_computation.6 | convolution fusion | flops 135790080 | bytes 4392960 | tf_op jit(solution)/shard_map/cond/branch_1_fun/qhmd,khmd->hmqk/dot_general | solution.py:29
  158.7 0.4 copy-done.1
  159.1 4.8 %fusion = f32[4,2,64,256]{3,2,1,0:T(8,128)S(1)} fusion(f32[1024,4,256]{0,2,1:T(8,128)S(1)} %copy-done.1, f32[4,2,64,1024]{3,2,1,0:T(8,128)S(1)} %get-tuple-element.61, f32[4,2,64]{2,1,0:T(2,128)S(1)} %broadcast_maximum_fusion, pred[64,1024]{1,0:T(8,128)(4,1)S(1)} %broadcast_compare_fusion), kind=kOutput, calls=%fused_computation.2 | convolution fusion | flops 1612709888 | bytes 6883328 | tf_op jit(solution)/shard_map/cond/branch_1_fun/hmqk,khd->hmqd/dot_general | solution.py:36
  164.0 0.7 fusion.3
  164.7 0.0 reduce-scatter.2.cloned.1.call-done
  164.7 3.5 %all-to-all-start.1 = ((bf16[1024,8,32]{0,2,1:T(8,128)(2,1)}), bf16[1024,8,32]{0,2,1:T(8,128)(2,1)S(1)}, u32[]{:S(2)}, u32[]{:S(2)}) async-start(bf16[1024,8,32]{0,2,1:T(8,128)(2,1)} %bitcast.101), calls=%async_computation.2 | async-start | bytes 1048576 | tf_op jit(solution)/shard_map/all_to_all | solution.py:145
  168.2 0.0 copy-done.7
  168.3 0.4 multiply_reduce_fusion.1
  168.6 0.0 copy-done.6
  168.6 0.1 fusion.60
  168.8 0.7 pad_maximum_fusion
  169.5 12.6 %all-to-all-done.1 = bf16[1024,8,32]{0,2,1:T(8,128)(2,1)S(1)} async-done(((bf16[1024,8,32]{0,2,1:T(8,128)(2,1)}), bf16[1024,8,32]{0,2,1:T(8,128)(2,1)S(1)}, u32[]{:S(2)}, u32[]{:S(2)}) %all-to-all-start.1) | async-done | bytes 524320 | tf_op jit(solution)/shard_map/all_to_all | solution.py:145
  182.1 0.2 convolution_multiply_fusion.1
  182.4 0.9 fusion.41
  (25 shorter events, 0.2 us)
Async XLA Ops:
  8.0 6.0 %copy-start.2 = (bf16[64,4096]{1,0:T(8,128)(2,1)S(1)}, bf16[64,4096]{1,0:T(8,128)(2,1)}, u32[]{:S(2)}) copy-start(bf16[64,4096]{1,0:T(8,128)(2,1)} %param.21) | copy-start | bytes 1572868
  8.0 102.0 %all-gather.5.cloned.1.call-start = ((), (), s32[]{:S(2)}) async-start(), calls=%async_computation.4 | async-start | bytes 2359296 | tf_op jit(solution)/shard_map/all_gather | solution.py:79
  18.2 7.5 %copy-start.3 = (bf16[128,1024]{1,0:T(8,128)(2,1)S(1)}, bf16[128,1024]{1,0:T(8,128)(2,1)}, u32[]{:S(2)}) copy-start(bf16[128,1024]{1,0:T(8,128)(2,1)} %param.17) | copy-start | bytes 786436
  18.2 78.2 %all-to-all-start = ((bf16[8,32,4096]{2,1,0:T(8,128)(2,1)}), bf16[8,32,4096]{2,1,0:T(8,128)(2,1)S(1)}, u32[]{:S(2)}, u32[]{:S(2)}) async-start(bf16[8,32,4096]{2,1,0:T(8,128)(2,1)} %bitcast.20), calls=%async_computation | async-start | bytes 4194304 | tf_op jit(solution)/shard_map/all_to_all | solution.py:133
  25.6 121.7 %all-gather.3.cloned.1.call-start = ((), (), s32[]{:S(2)}) async-start(), calls=%async_computation.3 | async-start | bytes 2359296 | tf_op jit(solution)/shard_map/all_gather | solution.py:78
  26.5 138.2 %reduce-scatter.2.cloned.1.call-start = ((), (), s32[]{:S(2)}) async-start(), calls=%async_computation.5 | async-start | bytes 2621440 | tf_op jit(solution)/shard_map/reduce_scatter | solution.py:137
  107.2 2.5 %copy-start.5 = (f32[64,2]{0,1:T(2,128)S(1)}, f32[64,2]{0,1:T(2,128)}, u32[]{:S(2)}) copy-start(f32[64,2]{0,1:T(2,128)} %param.24) | copy-start | bytes 1540
  110.0 37.3 %copy-start.4 = (bf16[128,1024]{1,0:T(8,128)(2,1)S(1)}, bf16[128,1024]{1,0:T(8,128)(2,1)}, u32[]{:S(2)}) copy-start(bf16[128,1024]{1,0:T(8,128)(2,1)} %param.16) | copy-start | bytes 786436
  147.5 2.8 %copy-start = (f32[1024,4,256]{0,2,1:T(8,128)S(1)}, f32[1024,4,256]{0,2,1:T(8,128)}, u32[]{:S(2)}) copy-start(f32[1024,4,256]{0,2,1:T(8,128)} %get-tuple-element.53) | copy-start | bytes 12582916 | tf_op jit(solution)/shard_map/cond
  155.9 12.4 %copy-start.7 = (f32[4]{0:T(128)S(1)}, f32[4]{0:T(128)}, u32[]{:S(2)}) copy-start(f32[4]{0:T(128)} %param.19) | copy-start | bytes 52
  156.3 2.8 %copy-start.1 = (f32[1024,4,256]{0,2,1:T(8,128)S(1)}, f32[1024,4,256]{0,2,1:T(8,128)}, u32[]{:S(2)}) copy-start(f32[1024,4,256]{0,2,1:T(8,128)} %get-tuple-element.48) | copy-start | bytes 12582916 | tf_op jit(solution)/shard_map/cond
  164.7 4.0 %copy-start.6 = (f32[256]{0:T(256)S(1)}, f32[256]{0:T(256)}, u32[]{:S(2)}) copy-start(f32[256]{0:T(256)} %param.20) | copy-start | bytes 3076
  164.7 17.4 %all-to-all-start.1 = ((bf16[1024,8,32]{0,2,1:T(8,128)(2,1)}), bf16[1024,8,32]{0,2,1:T(8,128)(2,1)S(1)}, u32[]{:S(2)}, u32[]{:S(2)}) async-start(bf16[1024,8,32]{0,2,1:T(8,128)(2,1)} %bitcast.101), calls=%async_computation.2 | async-start | bytes 1048576 | tf_op jit(solution)/shard_map/all_to_all | solution.py:145
Sparse Core Ops, SparseCore 0:
  10.9 83.9 all-gather.4
  97.5 49.7 all-gather.2
Sparse Core Ops, SparseCore 1:
  107.3 30.1 reduce-scatter.1
where the time goes:
time: 191 us
  waiting for transfers between devices  116 us (61%)
  matrix products  26.5 us (14%)
  between operations  17.1 us (9%)
  starting transfers between devices  11 us (6%)
  local copies, waits for them, and re-layouts  10.5 us (5%)
  other arithmetic  9.63 us (5%)
    all_to_all x1, waiting for transfers between devices, local(): lax.all_to_all(outgoing, 'ep', split_axis=0, concat_axis=0, tiled=True)  69.8 us
    all_gather x1, waiting for transfers between devices, local(): key_block = lax.all_gather(key_rows, 'ep', axis=0, tiled=True)  33.2 us
    all_to_all x1, waiting for transfers between devices, local(): lax.all_to_all(summed, 'ep', split_axis=1, concat_axis=1, tiled=True)  12.6 us
    dot_general x2, matrix products, fold_block(): jnp.einsum('hmqk,khd->hmqd', weights, value_heads, precision=lax.Precisio...  9.67 us
    all_to_all x1, starting transfers between devices, local(): lax.all_to_all(outgoing, 'ep', split_axis=0, concat_axis=0, tiled=True)  7.41 us
    dot_general x1, matrix products, local(): lax.dot_general(down_local, hidden, (((0,), (1,)), ((), ())), preferred_e...  7.37 us
    dot_general x2, matrix products, fold_block(): jnp.einsum('qhmd,khmd->hmqk', query_group, key_heads, preferred_element_t...  4.85 us
    convert_element_type x1, other arithmetic, local(): value_block.reshape(key_count, head_local, VD).astype(jnp.float32)  4.08 us
  transfers between devices with their start and end apart: 5, of which 3 were waited for; matrix products, arithmetic and copies ran while one was open for 22% of the time, Pallas kernels for 0%

commit v1 on v0

--- a/solution.py
+++ b/solution.py
@@ -1,6 +1,10 @@
+import functools
+
 import jax
 import jax.numpy as jnp
 from jax import lax
+from jax.experimental import pallas as pl
+from jax.experimental.pallas import tpu as pltpu
 from jax.sharding import PartitionSpec as P
 
 QKD = 128
@@ -40,7 +44,7 @@
     return (new_max, denominators, accumulated)
 
 
-def local(
+def local_general(
     queries,
     key_rows,
     values,
@@ -155,9 +159,392 @@
     return (attended, expert_out)
 
 
+MESH = pl.DeviceIdType.MESH
+
+
+def step_kernel(
+    n,
+    heads,
+    q_ref,
+    k_ref,
+    v_ref,
+    lam_ref,
+    gain_ref,
+    tok_ref,
+    pick_ref,
+    gate_ref,
+    wg_ref,
+    wu_ref,
+    wd_ref,
+    att_ref,
+    out_ref,
+    wg,
+    wu,
+    wd,
+    qbuf,
+    kbuf,
+    vbuf,
+    osend,
+    oret,
+    arr,
+    part,
+    near,
+    csum,
+    far,
+    res,
+    ret,
+    w_sem,
+    tok_send,
+    tok_recv,
+    ty_send,
+    ty_recv,
+    tc_send,
+    tc_recv,
+    a_send,
+    a_recv,
+    o_send,
+    o_recv,
+    rc_send,
+    rc_recv,
+    ry_send,
+    ry_recv,
+    e_send,
+    e_recv,
+):
+    me = lax.axis_index("ep")
+    tp = lax.axis_index("tp")
+    y = tp // 2
+    core = tp % 2
+    tp_core = y * 2 + 1 - core
+    tp_y = (1 - y) * 2 + core
+    rows, slots, width = q_ref.shape[0], tok_ref.shape[1], tok_ref.shape[2]
+
+    def peer(j):
+        return lax.rem(me + j, n)
+
+    def source(j):
+        return lax.rem(me + n - j, n)
+
+    def remote(src, dst, send, recv, ep, tpi):
+        return pltpu.make_async_remote_copy(
+            src_ref=src,
+            dst_ref=dst,
+            send_sem=send,
+            recv_sem=recv,
+            device_id=(ep, tpi),
+            device_id_type=MESH,
+        )
+
+    loads = [
+        pltpu.make_async_copy(wg_ref.at[0], wg, w_sem.at[0]),
+        pltpu.make_async_copy(wu_ref.at[0], wu, w_sem.at[1]),
+        pltpu.make_async_copy(wd_ref.at[0], wd, w_sem.at[2]),
+    ]
+    for load in loads:
+        load.start()
+
+    barrier = pltpu.get_barrier_semaphore()
+    for j in range(1, n):
+        pl.semaphore_signal(barrier, inc=1, device_id=(peer(j), tp), device_id_type=MESH)
+    pl.semaphore_signal(barrier, inc=1, device_id=(me, tp_core), device_id_type=MESH)
+    pl.semaphore_signal(barrier, inc=1, device_id=(me, tp_y), device_id_type=MESH)
+    pl.semaphore_wait(barrier, n + 1)
+
+    sent = []
+    tok_copies = []
+    for j in range(1, n):
+        c = remote(
+            tok_ref.at[peer(j)], arr.at[tp, me], tok_send.at[j], tok_recv.at[j], peer(j), tp
+        )
+        c.start()
+        tok_copies.append(c)
+    unit_copies = []
+    for j in range(1, n):
+        d = peer(j)
+        cols = pl.ds(pl.multiple_of(d * QKD, QKD), QKD)
+        vcols = pl.ds(pl.multiple_of((d // 2) * VD, VD), VD)
+        group = [
+            remote(q_ref.at[:, cols], qbuf.at[me], a_send.at[0, j], a_recv.at[0, j], d, tp),
+            remote(k_ref.at[:, cols], kbuf.at[me], a_send.at[1, j], a_recv.at[1, j], d, tp),
+            remote(v_ref.at[:, vcols], vbuf.at[me], a_send.at[2, j], a_recv.at[2, j], d, tp),
+        ]
+        for c in group:
+            c.start()
+        unit_copies.append(group)
+    own = pl.ds(pl.multiple_of(me * QKD, QKD), QKD)
+    own_v = pl.ds(pl.multiple_of((me // 2) * VD, VD), VD)
+    qbuf[me] = q_ref[:, own]
+    kbuf[me] = k_ref[:, own]
+    vbuf[me] = v_ref[:, own_v]
+
+    y_copies, core_copies = [], []
+    for j in range(n):
+        s = source(j)
+        if j == 0:
+            src = tok_ref.at[me]
+            arr[tp, me] = tok_ref[me]
+        else:
+            tok_copies[j - 1].wait_recv()
+            src = arr.at[tp, s]
+        c = remote(src, arr.at[tp, s], ty_send.at[j], ty_recv.at[j], me, tp_y)
+        c.start()
+        y_copies.append(c)
+        c = remote(src, arr.at[tp, s], tc_send.at[0, j], tc_recv.at[0, j], me, tp_core)
+        c.start()
+        core_copies.append(c)
+    for j in range(n):
+        s = source(j)
+        y_copies[j].wait_recv()
+        c = remote(
+            arr.at[tp_y, s], arr.at[tp_y, s], tc_send.at[1, j], tc_recv.at[1, j], me, tp_core
+        )
+        c.start()
+        core_copies.append(c)
+    for c in core_copies:
+        c.wait_recv()
+    sent += tok_copies + y_copies + core_copies
+
+    for load in loads:
+        load.wait()
+    total = n * slots
+    gate = jnp.zeros((total, wg.shape[1]), jnp.float32)
+    up = jnp.zeros((total, wg.shape[1]), jnp.float32)
+    for i in range(4):
+        a = arr[i].reshape(total, width)
+        gate += jnp.dot(
+            a, wg[i * width : (i + 1) * width, :], preferred_element_type=jnp.float32
+        )
+        up += jnp.dot(a, wu[i * width : (i + 1) * width, :], preferred_element_type=jnp.float32)
+    hidden = (jax.nn.silu(gate) * up).astype(jnp.bfloat16)
+    order = (tp_y + 1 - 2 * core, tp_y, tp_core, tp)
+    near_copies = []
+    for i in range(4):
+        cols = pl.ds(pl.multiple_of(order[i] * width, width), width)
+        part[i] = (
+            jnp.dot(hidden, wd[:, cols], preferred_element_type=jnp.float32)
+            .astype(jnp.bfloat16)
+            .reshape(n, slots, width)
+        )
+        if i % 2 == 0:
+            h = i // 2
+            c = remote(part.at[i], near.at[h], rc_send.at[h], rc_recv.at[h], me, tp_core)
+            c.start()
+            near_copies.append(c)
+    near_copies[0].wait_recv()
+    far_copies = []
+    for j in range(n):
+        d = peer(j)
+        csum[d] = (part[1, d].astype(jnp.float32) + near[0, d].astype(jnp.float32)).astype(
+            jnp.bfloat16
+        )
+        c = remote(csum.at[d], far.at[d], ry_send.at[j], ry_recv.at[j], me, tp_y)
+        c.start()
+        far_copies.append(c)
+    sent += near_copies + far_copies
+
+    for group in unit_copies:
+        for c in group:
+            c.wait_recv()
+        sent += group
+    blk = 2
+    size = blk * rows
+    diag = (
+        lax.broadcasted_iota(jnp.int32, (size, size), 1)
+        <= lax.broadcasted_iota(jnp.int32, (size, size), 0)
+    )
+    for i in range(n // blk):
+        seen = (i + 1) * size
+        q = qbuf[i * blk : (i + 1) * blk].reshape(size, QKD)
+        k = kbuf[0 : (i + 1) * blk].reshape(seen, QKD)
+        v = vbuf[0 : (i + 1) * blk].reshape(seen, VD)
+        scores = lax.dot_general(
+            q, k, (((1,), (1,)), ((), ())), preferred_element_type=jnp.float32
+        ) * QKD ** (-0.5)
+        last = jnp.where(diag, scores[:, i * size :], neg_big)
+        scores = last if i == 0 else jnp.concatenate([scores[:, : i * size], last], axis=1)
+        weights = jnp.exp(scores - jnp.max(scores, axis=-1, keepdims=True))
+        bottom = jnp.sum(weights, axis=-1, keepdims=True)
+        o = jnp.dot(weights.astype(jnp.bfloat16), v, preferred_element_type=jnp.float32) / bottom
+        osend[i * blk : (i + 1) * blk] = o.astype(jnp.bfloat16).reshape(blk, rows, VD)
+        for s in range(i * blk, (i + 1) * blk):
+
+            @pl.when(s != me)
+            def _(s=s):
+                remote(
+                    osend.at[s], oret.at[me], o_send.at[s], o_recv.at[me], s, tp
+                ).start()
+
+    near_copies[1].wait_recv()
+    back_copies = []
+    for j in range(n):
+        d = peer(j)
+        far_copies[j].wait_recv()
+        val = (
+            part[3, d].astype(jnp.float32)
+            + near[1, d].astype(jnp.float32)
+            + far[d].astype(jnp.float32)
+        ).astype(jnp.bfloat16)
+        if j == 0:
+            ret[me] = val
+        else:
+            res[d] = val
+            c = remote(res.at[d], ret.at[me], e_send.at[j], e_recv.at[j], d, tp)
+            c.start()
+            back_copies.append(c)
+
+    oret[me] = osend[me]
+    for u in range(n):
+
+        @pl.when(u != me)
+        def _(u=u):
+            remote(osend.at[u], oret.at[u], o_send.at[u], o_recv.at[u], u, tp).wait()
+
+    for h in range(heads):
+        mixed = oret[2 * h].astype(jnp.float32) - lam_ref[h] * oret[2 * h + 1].astype(jnp.float32)
+        scaled = mixed * lax.rsqrt(jnp.mean(mixed * mixed, axis=-1, keepdims=True) + head_eps)
+        att_ref[:, h * VD : (h + 1) * VD] = (scaled * gain_ref[...] * head_scale).astype(
+            jnp.bfloat16
+        )
+
+    for c in back_copies:
+        c.wait_recv()
+    sent += back_copies
+    returned = ret[...].reshape(total, width)
+    combined = jnp.zeros(out_ref.shape, jnp.float32)
+    for i in range(TOP):
+        picked = jnp.dot(pick_ref[i], returned, preferred_element_type=jnp.float32)
+        combined = combined + gate_ref[:, i : i + 1] * picked
+    out_ref[...] = combined.astype(jnp.bfloat16)
+    for c in sent:
+        c.wait_send()
+
+
+def local(
+    queries,
+    key_rows,
+    values,
+    lambdas,
+    head_gain,
+    tokens,
+    moe_gain,
+    routes,
+    route_scores,
+    w_gate,
+    w_up,
+    w_down,
+):
+    n = lax.axis_size("ep")
+    heads = lambdas.shape[0]
+    rows = queries.shape[0]
+    rows_b, model = tokens.shape
+    slots = 2 * TOP * rows_b // n
+    width = model // 4
+    ff = w_gate.shape[2]
+    token_f32 = tokens.astype(jnp.float32)
+    normed = (
+        token_f32
+        * lax.rsqrt(jnp.mean(token_f32 * token_f32, axis=-1, keepdims=True) + moe_eps)
+        * moe_gain
+    ).astype(jnp.bfloat16)
+    gate_weights = jax.nn.softmax(route_scores, axis=-1)
+    flat = routes.reshape(-1)
+    count = flat.shape[0]
+    place = jnp.arange(count, dtype=jnp.int32)
+    earlier = (flat[:, None] == flat[None, :]) & (place[None, :] < place[:, None])
+    slot_of = (flat * slots + jnp.sum(earlier.astype(jnp.int32), axis=1)).reshape(routes.shape)
+    ids = jnp.arange(n * slots, dtype=jnp.int32)
+    pick = (slot_of.T[:, :, None] == ids[None, None, :]).astype(jnp.bfloat16)
+    mine = lax.dynamic_slice_in_dim(normed, lax.axis_index("tp") * width, width, 1)
+    outgoing = (
+        lax.dot_general(
+            pick[0] + pick[1], mine, (((0,), (0,)), ((), ())), preferred_element_type=jnp.float32
+        )
+        .astype(jnp.bfloat16)
+        .reshape(n, slots, width)
+    )
+    vmem = pl.BlockSpec(memory_space=pltpu.VMEM)
+    hbm = pl.BlockSpec(memory_space=pl.ANY)
+    smem = pl.BlockSpec(memory_space=pltpu.SMEM)
+    bf16 = jnp.bfloat16
+    dma = pltpu.SemaphoreType.DMA
+    return tuple(
+        pl.pallas_call(
+            functools.partial(step_kernel, n, heads),
+            out_shape=(
+                jax.ShapeDtypeStruct(queries.shape, bf16),
+                jax.ShapeDtypeStruct((rows_b, width), bf16),
+            ),
+            in_specs=[vmem, vmem, vmem, smem, vmem, vmem, vmem, vmem, hbm, hbm, hbm],
+            out_specs=(vmem, vmem),
+            scratch_shapes=[
+                pltpu.VMEM((model, ff), bf16),
+                pltpu.VMEM((model, ff), bf16),
+                pltpu.VMEM((ff, model), bf16),
+                pltpu.VMEM((n, rows, QKD), bf16),
+                pltpu.VMEM((n, rows, QKD), bf16),
+                pltpu.VMEM((n, rows, VD), bf16),
+                pltpu.VMEM((n, rows, VD), bf16),
+                pltpu.VMEM((n, rows, VD), bf16),
+                pltpu.VMEM((4, n, slots, width), bf16),
+                pltpu.VMEM((4, n, slots, width), bf16),
+                pltpu.VMEM((2, n, slots, width), bf16),
+                pltpu.VMEM((n, slots, width), bf16),
+                pltpu.VMEM((n, slots, width), bf16),
+                pltpu.VMEM((n, slots, width), bf16),
+                pltpu.VMEM((n, slots, width), bf16),
+                dma((3,)),
+                dma((n,)),
+                dma((n,)),
+                dma((n,)),
+                dma((n,)),
+                dma((2, n)),
+                dma((2, n)),
+                dma((3, n)),
+                dma((3, n)),
+                dma((n,)),
+                dma((n,)),
+                dma((2,)),
+                dma((2,)),
+                dma((n,)),
+                dma((n,)),
+                dma((n,)),
+                dma((n,)),
+            ],
+            compiler_params=pltpu.CompilerParams(
+                collective_id=0, has_side_effects=True, vmem_limit_bytes=56 * 1024 * 1024
+            ),
+        )(
+            queries,
+            key_rows,
+            values,
+            lambdas,
+            head_gain[None, :],
+            outgoing,
+            pick,
+            gate_weights,
+            w_gate,
+            w_up,
+            w_down,
+        )
+    )
+
+
+def fits(mesh, head_count):
+    n, parts = mesh.shape["ep"], mesh.shape["tp"]
+    return parts == 4 and n % 2 == 0 and 2 * (head_count // parts) == n
+
+
 def solution(mesh):
+    def step(*args):
+        body = local if fits(mesh, args[3].shape[0]) else local_general
+        return sharded(mesh, body)(*args)
+
+    return step
+
+
+def sharded(mesh, body):
     return jax.shard_map(
-        local,
+        body,
         mesh=mesh,
         in_specs=(
             P("ep", "tp"),

time: 191 us -> 80.2 us (0.42)
  the two profiles are of different devices: /device:TPU:0 before, /device:TPU:24 now
where the time goes in v1:
time: 80.2 us; the launch traced here: 78.6 us
  Pallas kernels  66.2 us (83%)
  other arithmetic  5.44 us (7%)
  local copies, waits for them, and re-layouts  5.14 us (6%)
  matrix products  1.15 us (1%)
    pallas_call x1, Pallas kernels, local(): pl.pallas_call(functools.partial(step_kernel, n, heads), out_shape=(jax.S...  66.2 us
    unnamed x5, local copies, waits for them, and re-layouts  4.01 us

profile of v1, /device:TPU:24, one launch (start us, length us, event | category | flops | bytes accessed | tf_op | source)
XLA Modules:
  0.0 78.6 jit_solution(2101672732689384578)
XLA Ops:
  0.6 0.7 dynamic-slice
  1.3 0.8 copy.32
  2.1 0.1 eq.28
  2.2 0.2 convert_reduce_fusion
  2.4 0.1 reduce_sum.30
  2.6 0.1 copy.33
  2.6 0.7 add_bitcast_fusion
  3.3 0.1 fusion.5.pick_ref
  3.4 0.0 copy-start
  3.4 1.1 %convert_element_type.17 = f32[64,4096]{1,0:T(8,128)S(1)} convert(bf16[64,4096]{1,0:T(8,128)(2,1)} %param.17) | non-fusion elementwise | flops 262144 | bytes 1572864 | tf_op jit(solution)/shard_map/convert_element_type | solution.py:443
  4.6 1.2 %multiply_reduce_fusion = f32[64]{0:T(128)S(1)} fusion(bf16[64,4096]{1,0:T(8,128)(2,1)} %param.17), kind=kLoop, calls=%fused_computation.1 | loop fusion | flops 786368 | bytes 524544 | tf_op jit(solution)/shard_map/reduce_sum | solution.py:446
  5.8 1.2 %convolution_convert_fusion = bf16[256,1024]{1,0:T(8,128)(2,1)} fusion(f32[64,4096]{1,0:T(8,128)S(1)} %convert_element_type.17, s32[]{:T(128)S(6)} %select_n.3, f32[1024]{0:T(1024)S(1)} %dynamic-slice, f32[64]{0:T(128)S(1)} %add_rsqrt_fusion, bf16[2,64,256]{2,1,0:T(8,128)(2,1)S(1)} %fusion.5.pick_ref), kind=kOutput, calls=%fused_computation | convolution fusion | flops 34029568 | bytes 856580 | tf_op jit(solution)/shard_map/dot_general | solution.py:459
  7.0 0.7 reduce_max.9
  7.7 0.7 fusion.11
  8.4 0.1 copy.34
  8.5 0.7 broadcast_divide_fusion.gate_ref
  9.2 0.0 copy-done
  9.2 66.2 %shard_map.131 = (bf16[128,1024]{1,0:T(8,128)(2,1)}, bf16[64,1024]{1,0:T(8,128)(2,1)}) custom-call(bf16[128,1024]{1,0:T(8,128)(2,1)} %q_ref.1, bf16[128,1024]{1,0:T(8,128)(2,1)} %k_ref.1, bf16[128,1024]{1,0:T(8,128)(2,1)} %v_ref.1, f32[4]{0:T(128)} %lam_ref.1, f32[1,256]{1,0:T(1,128)} %bitcast.8, bf16[8,32,1024]{2,1,0:T(8,128)(2,1)} %bitcast.7, ...), custom_call_target="tpu_custom_call" | custom-call | tf_op jit(solution)/shard_map/pallas_call | solution.py:471
  75.4 1.7 %copy.37 = bf16[128,1024]{1,0:T(8,128)(2,1)} copy(bf16[128,1024]{1,0:T(8,128)(2,1)} %get-tuple-element.6) | data formatting | bytes 524288
  77.0 1.6 %copy.38 = bf16[64,1024]{1,0:T(8,128)(2,1)} copy(bf16[64,1024]{1,0:T(8,128)(2,1)} %get-tuple-element.7) | data formatting | bytes 262144
  (1 shorter events, 0.0 us)
Async XLA Ops:
  3.4 5.8 %copy-start = (bf16[2,64,256]{2,1,0:T(8,128)(2,1)}, bf16[2,64,256]{2,1,0:T(8,128)(2,1)S(1)}, u32[]{:S(2)}) copy-start(bf16[2,64,256]{2,1,0:T(8,128)(2,1)S(1)} %fusion.5.pick_ref) | copy-start | bytes 196612

commit v2 on v1

--- a/solution.py
+++ b/solution.py
@@ -170,9 +170,10 @@
     v_ref,
     lam_ref,
     gain_ref,
-    tok_ref,
-    pick_ref,
-    gate_ref,
+    tokens_ref,
+    moe_gain_ref,
+    routes_ref,
+    score_ref,
     wg_ref,
     wu_ref,
     wd_ref,
@@ -186,6 +187,10 @@
     vbuf,
     osend,
     oret,
+    fin,
+    att_in,
+    pick,
+    tok,
     arr,
     part,
     near,
@@ -202,8 +207,12 @@
     tc_recv,
     a_send,
     a_recv,
+    v_send,
+    v_recv,
     o_send,
     o_recv,
+    f_send,
+    f_recv,
     rc_send,
     rc_recv,
     ry_send,
@@ -217,7 +226,14 @@
     core = tp % 2
     tp_core = y * 2 + 1 - core
     tp_y = (1 - y) * 2 + core
-    rows, slots, width = q_ref.shape[0], tok_ref.shape[1], tok_ref.shape[2]
+    tp_both = (1 - y) * 2 + 1 - core
+    side = me % 2
+    head = me // 2
+    pair = head * 2 + 1 - side
+    rows = q_ref.shape[0]
+    rows_b = tokens_ref.shape[0]
+    _, slots, width = tok.shape
+    total = n * slots
 
     def peer(j):
         return lax.rem(me + j, n)
@@ -235,6 +251,11 @@
             device_id_type=MESH,
         )
 
+    barrier = pltpu.get_barrier_semaphore()
+    for j in range(1, n):
+        pl.semaphore_signal(barrier, inc=1, device_id=(peer(j), tp), device_id_type=MESH)
+    pl.semaphore_signal(barrier, inc=1, device_id=(me, tp_core), device_id_type=MESH)
+    pl.semaphore_signal(barrier, inc=1, device_id=(me, tp_y), device_id_type=MESH)
     loads = [
         pltpu.make_async_copy(wg_ref.at[0], wg, w_sem.at[0]),
         pltpu.make_async_copy(wu_ref.at[0], wu, w_sem.at[1]),
@@ -243,46 +264,67 @@
     for load in loads:
         load.start()
 
-    barrier = pltpu.get_barrier_semaphore()
-    for j in range(1, n):
-        pl.semaphore_signal(barrier, inc=1, device_id=(peer(j), tp), device_id_type=MESH)
-    pl.semaphore_signal(barrier, inc=1, device_id=(me, tp_core), device_id_type=MESH)
-    pl.semaphore_signal(barrier, inc=1, device_id=(me, tp_y), device_id_type=MESH)
+    features = pl.ds(pl.multiple_of(tp * width, width), width)
+    token_f32 = tokens_ref[...].astype(jnp.float32)
+    inverse = lax.rsqrt(jnp.mean(token_f32 * token_f32, axis=-1, keepdims=True) + moe_eps)
+    normed = (
+        tokens_ref[:, features].astype(jnp.float32) * inverse * moe_gain_ref[:, features]
+    ).astype(jnp.bfloat16)
+    lane = lax.broadcasted_iota(jnp.int32, (rows_b, 128), 1)
+    named = [routes_ref[:, c : c + 1] == lane for c in range(TOP)]
+    either = jnp.where(named[0] | named[1], 1.0, 0.0).astype(jnp.bfloat16)
+    square = (rows_b, rows_b)
+    below = jnp.where(
+        lax.broadcasted_iota(jnp.int32, square, 1) < lax.broadcasted_iota(jnp.int32, square, 0),
+        1.0,
+        0.0,
+    ).astype(jnp.bfloat16)
+    before = jnp.dot(below, either, preferred_element_type=jnp.float32)
+    slot_ids = lax.broadcasted_iota(jnp.int32, (rows_b, total), 1).astype(jnp.float32)
+    chosen = jnp.zeros((rows_b, total), jnp.float32)
+    for c in range(TOP):
+        position = jnp.sum(jnp.where(named[c], before, 0.0), axis=1, keepdims=True)
+        slot = routes_ref[:, c : c + 1].astype(jnp.float32) * slots + position
+        hit = jnp.where(slot == slot_ids, 1.0, 0.0)
+        pick[c] = hit.astype(jnp.bfloat16)
+        chosen = chosen + hit
+    tok[...] = (
+        jnp.dot(chosen.T.astype(jnp.bfloat16), normed, preferred_element_type=jnp.float32)
+        .astype(jnp.bfloat16)
+        .reshape(n, slots, width)
+    )
     pl.semaphore_wait(barrier, n + 1)
 
     sent = []
     tok_copies = []
     for j in range(1, n):
-        c = remote(
-            tok_ref.at[peer(j)], arr.at[tp, me], tok_send.at[j], tok_recv.at[j], peer(j), tp
-        )
+        c = remote(tok.at[peer(j)], arr.at[tp, me], tok_send.at[j], tok_recv.at[j], peer(j), tp)
         c.start()
         tok_copies.append(c)
-    unit_copies = []
-    for j in range(1, n):
-        d = peer(j)
-        cols = pl.ds(pl.multiple_of(d * QKD, QKD), QKD)
-        vcols = pl.ds(pl.multiple_of((d // 2) * VD, VD), VD)
-        group = [
-            remote(q_ref.at[:, cols], qbuf.at[me], a_send.at[0, j], a_recv.at[0, j], d, tp),
-            remote(k_ref.at[:, cols], kbuf.at[me], a_send.at[1, j], a_recv.at[1, j], d, tp),
-            remote(v_ref.at[:, vcols], vbuf.at[me], a_send.at[2, j], a_recv.at[2, j], d, tp),
-        ]
-        for c in group:
+    unit_copies = {}
+    for which, src, dst in ((0, v_ref, None), (1, k_ref, kbuf.at[me]), (2, q_ref, qbuf.at[me])):
+        for j in range(1, n):
+            d = peer(j)
+            cols = pl.ds(pl.multiple_of(d * QKD, QKD), QKD)
+            to = vbuf.at[d % 2, me] if which == 0 else dst
+            c = remote(src.at[:, cols], to, a_send.at[which, j], a_recv.at[which, j], d, tp)
             c.start()
-        unit_copies.append(group)
+            unit_copies[which, j] = c
     own = pl.ds(pl.multiple_of(me * QKD, QKD), QKD)
-    own_v = pl.ds(pl.multiple_of((me // 2) * VD, VD), VD)
     qbuf[me] = q_ref[:, own]
     kbuf[me] = k_ref[:, own]
-    vbuf[me] = v_ref[:, own_v]
-
-    y_copies, core_copies = [], []
+    vbuf[side, me] = v_ref[:, own]
+    v_copies = [
+        remote(v_ref.at[:, own], vbuf.at[side, me], v_send.at[me], v_recv.at[me], pair, tp)
+    ]
+    v_copies[0].start()
+
+    y_copies, core_copies = [], ([], [])
     for j in range(n):
         s = source(j)
         if j == 0:
-            src = tok_ref.at[me]
-            arr[tp, me] = tok_ref[me]
+            src = tok.at[me]
+            arr[tp, me] = tok[me]
         else:
             tok_copies[j - 1].wait_recv()
             src = arr.at[tp, s]
@@ -291,7 +333,23 @@
         y_copies.append(c)
         c = remote(src, arr.at[tp, s], tc_send.at[0, j], tc_recv.at[0, j], me, tp_core)
         c.start()
-        core_copies.append(c)
+        core_copies[0].append(c)
+
+    def first_products(quarter):
+        a = arr[quarter].reshape(total, width)
+        deep = pl.ds(pl.multiple_of(quarter * width, width), width)
+        return (
+            jnp.dot(a, wg[deep, :], preferred_element_type=jnp.float32),
+            jnp.dot(a, wu[deep, :], preferred_element_type=jnp.float32),
+        )
+
+    loads[0].wait()
+    loads[1].wait()
+    gate, up = first_products(tp)
+    for c in core_copies[0]:
+        c.wait_recv()
+    more = first_products(tp_core)
+    gate, up = gate + more[0], up + more[1]
     for j in range(n):
         s = source(j)
         y_copies[j].wait_recv()
@@ -299,24 +357,18 @@
             arr.at[tp_y, s], arr.at[tp_y, s], tc_send.at[1, j], tc_recv.at[1, j], me, tp_core
         )
         c.start()
-        core_copies.append(c)
-    for c in core_copies:
+        core_copies[1].append(c)
+    more = first_products(tp_y)
+    gate, up = gate + more[0], up + more[1]
+    for c in core_copies[1]:
         c.wait_recv()
-    sent += tok_copies + y_copies + core_copies
-
-    for load in loads:
-        load.wait()
-    total = n * slots
-    gate = jnp.zeros((total, wg.shape[1]), jnp.float32)
-    up = jnp.zeros((total, wg.shape[1]), jnp.float32)
-    for i in range(4):
-        a = arr[i].reshape(total, width)
-        gate += jnp.dot(
-            a, wg[i * width : (i + 1) * width, :], preferred_element_type=jnp.float32
-        )
-        up += jnp.dot(a, wu[i * width : (i + 1) * width, :], preferred_element_type=jnp.float32)
+    more = first_products(tp_both)
+    gate, up = gate + more[0], up + more[1]
+    sent += tok_copies + y_copies + core_copies[0] + core_copies[1]
     hidden = (jax.nn.silu(gate) * up).astype(jnp.bfloat16)
-    order = (tp_y + 1 - 2 * core, tp_y, tp_core, tp)
+
+    loads[2].wait()
+    order = (tp_both, tp_y, tp_core, tp)
     near_copies = []
     for i in range(4):
         cols = pl.ds(pl.multiple_of(order[i] * width, width), width)
@@ -341,42 +393,32 @@
         c.start()
         far_copies.append(c)
     sent += near_copies + far_copies
-
-    for group in unit_copies:
-        for c in group:
-            c.wait_recv()
-        sent += group
-    blk = 2
-    size = blk * rows
+    near_copies[1].wait_recv()
+
+    for j in range(1, n):
+        s = source(j)
+        unit_copies[0, j].wait_recv()
+        c = remote(vbuf.at[side, s], vbuf.at[side, s], v_send.at[s], v_recv.at[s], pair, tp)
+        c.start()
+        v_copies.append(c)
+    for j in range(1, n):
+        unit_copies[1, j].wait_recv()
+        unit_copies[2, j].wait_recv()
+    for c in v_copies:
+        c.wait_recv()
+    sent += list(unit_copies.values()) + v_copies
+
+    lam = lam_ref[head]
+    keep = jnp.where(side == 0, 1.0, -lam)
+    take = jnp.where(side == 0, -lam, 1.0)
+    size = 2 * rows
     diag = (
         lax.broadcasted_iota(jnp.int32, (size, size), 1)
         <= lax.broadcasted_iota(jnp.int32, (size, size), 0)
     )
-    for i in range(n // blk):
-        seen = (i + 1) * size
-        q = qbuf[i * blk : (i + 1) * blk].reshape(size, QKD)
-        k = kbuf[0 : (i + 1) * blk].reshape(seen, QKD)
-        v = vbuf[0 : (i + 1) * blk].reshape(seen, VD)
-        scores = lax.dot_general(
-            q, k, (((1,), (1,)), ((), ())), preferred_element_type=jnp.float32
-        ) * QKD ** (-0.5)
-        last = jnp.where(diag, scores[:, i * size :], neg_big)
-        scores = last if i == 0 else jnp.concatenate([scores[:, : i * size], last], axis=1)
-        weights = jnp.exp(scores - jnp.max(scores, axis=-1, keepdims=True))
-        bottom = jnp.sum(weights, axis=-1, keepdims=True)
-        o = jnp.dot(weights.astype(jnp.bfloat16), v, preferred_element_type=jnp.float32) / bottom
-        osend[i * blk : (i + 1) * blk] = o.astype(jnp.bfloat16).reshape(blk, rows, VD)
-        for s in range(i * blk, (i + 1) * blk):
-
-            @pl.when(s != me)
-            def _(s=s):
-                remote(
-                    osend.at[s], oret.at[me], o_send.at[s], o_recv.at[me], s, tp
-                ).start()
-
-    near_copies[1].wait_recv()
     back_copies = []
-    for j in range(n):
+
+    def expert_back(j):
         d = peer(j)
         far_copies[j].wait_recv()
         val = (
@@ -392,31 +434,79 @@
             c.start()
             back_copies.append(c)
 
-    oret[me] = osend[me]
-    for u in range(n):
-
-        @pl.when(u != me)
-        def _(u=u):
-            remote(osend.at[u], oret.at[u], o_send.at[u], o_recv.at[u], u, tp).wait()
+    swaps = []
+
+    def finish(i):
+        s = 2 * i + side
+        swaps[i].wait_recv()
+        mixed = keep * osend[s].astype(jnp.float32) + take * oret[i].astype(jnp.float32)
+        scaled = mixed * lax.rsqrt(jnp.mean(mixed * mixed, axis=-1, keepdims=True) + head_eps)
+        fin[i] = (scaled * gain_ref[...] * head_scale).astype(jnp.bfloat16)
+
+        @pl.when(s != me)
+        def _():
+            remote(fin.at[i], att_in.at[head], f_send.at[i], f_recv.at[head], s, tp).start()
+
+        @pl.when(s == me)
+        def _():
+            att_in[head] = fin[i]
+
+    for i in range(n // 2):
+        seen = (i + 1) * size
+        q = qbuf[2 * i : 2 * i + 2].reshape(size, QKD)
+        k = kbuf[0 : 2 * i + 2].reshape(seen, QKD)
+        v = jnp.concatenate(
+            [vbuf[half, 0 : 2 * i + 2].reshape(seen, VD // 2) for half in range(2)], axis=1
+        )
+        scores = lax.dot_general(
+            q, k, (((1,), (1,)), ((), ())), preferred_element_type=jnp.float32
+        ) * QKD ** (-0.5)
+        last = jnp.where(diag, scores[:, i * size :], neg_big)
+        scores = last if i == 0 else jnp.concatenate([scores[:, : i * size], last], axis=1)
+        weights = jnp.exp(scores - jnp.max(scores, axis=-1, keepdims=True))
+        bottom = jnp.sum(weights, axis=-1, keepdims=True)
+        o = jnp.dot(weights.astype(jnp.bfloat16), v, preferred_element_type=jnp.float32) / bottom
+        osend[2 * i : 2 * i + 2] = o.astype(jnp.bfloat16).reshape(2, rows, VD)
+        c = remote(
+            osend.at[2 * i + 1 - side], oret.at[i], o_send.at[i], o_recv.at[i], pair, tp
+        )
+        c.start()
+        swaps.append(c)
+        expert_back(2 * i)
+        expert_back(2 * i + 1)
+        if i > 0:
+            finish(i - 1)
+    finish(n // 2 - 1)
+    sent += swaps + back_copies
 
     for h in range(heads):
-        mixed = oret[2 * h].astype(jnp.float32) - lam_ref[h] * oret[2 * h + 1].astype(jnp.float32)
-        scaled = mixed * lax.rsqrt(jnp.mean(mixed * mixed, axis=-1, keepdims=True) + head_eps)
-        att_ref[:, h * VD : (h + 1) * VD] = (scaled * gain_ref[...] * head_scale).astype(
-            jnp.bfloat16
-        )
+
+        @pl.when(2 * h + side != me)
+        def _(h=h):
+            remote(
+                fin.at[h], att_in.at[h], f_send.at[h], f_recv.at[h], 2 * h + side, tp
+            ).wait()
+
+        att_ref[:, h * VD : (h + 1) * VD] = att_in[h]
 
     for c in back_copies:
         c.wait_recv()
-    sent += back_copies
+    first, second = score_ref[:, 0:1], score_ref[:, 1:2]
+    top = jnp.maximum(first, second)
+    raised = (jnp.exp(first - top), jnp.exp(second - top))
     returned = ret[...].reshape(total, width)
     combined = jnp.zeros(out_ref.shape, jnp.float32)
-    for i in range(TOP):
-        picked = jnp.dot(pick_ref[i], returned, preferred_element_type=jnp.float32)
-        combined = combined + gate_ref[:, i : i + 1] * picked
+    for c in range(TOP):
+        picked = jnp.dot(pick[c], returned, preferred_element_type=jnp.float32)
+        combined = combined + raised[c] / (raised[0] + raised[1]) * picked
     out_ref[...] = combined.astype(jnp.bfloat16)
     for c in sent:
         c.wait_send()
+
+
+def hand_over(att_ref, out_ref, att_to, out_to):
+    att_to[...] = att_ref[...]
+    out_to[...] = out_ref[...]
 
 
 def local(
@@ -440,92 +530,83 @@
     slots = 2 * TOP * rows_b // n
     width = model // 4
     ff = w_gate.shape[2]
-    token_f32 = tokens.astype(jnp.float32)
-    normed = (
-        token_f32
-        * lax.rsqrt(jnp.mean(token_f32 * token_f32, axis=-1, keepdims=True) + moe_eps)
-        * moe_gain
-    ).astype(jnp.bfloat16)
-    gate_weights = jax.nn.softmax(route_scores, axis=-1)
-    flat = routes.reshape(-1)
-    count = flat.shape[0]
-    place = jnp.arange(count, dtype=jnp.int32)
-    earlier = (flat[:, None] == flat[None, :]) & (place[None, :] < place[:, None])
-    slot_of = (flat * slots + jnp.sum(earlier.astype(jnp.int32), axis=1)).reshape(routes.shape)
-    ids = jnp.arange(n * slots, dtype=jnp.int32)
-    pick = (slot_of.T[:, :, None] == ids[None, None, :]).astype(jnp.bfloat16)
-    mine = lax.dynamic_slice_in_dim(normed, lax.axis_index("tp") * width, width, 1)
-    outgoing = (
-        lax.dot_general(
-            pick[0] + pick[1], mine, (((0,), (0,)), ((), ())), preferred_element_type=jnp.float32
-        )
-        .astype(jnp.bfloat16)
-        .reshape(n, slots, width)
-    )
     vmem = pl.BlockSpec(memory_space=pltpu.VMEM)
     hbm = pl.BlockSpec(memory_space=pl.ANY)
     smem = pl.BlockSpec(memory_space=pltpu.SMEM)
     bf16 = jnp.bfloat16
     dma = pltpu.SemaphoreType.DMA
+    shapes = (
+        jax.ShapeDtypeStruct(queries.shape, bf16),
+        jax.ShapeDtypeStruct((rows_b, width), bf16),
+    )
+    held = pl.pallas_call(
+        functools.partial(step_kernel, n, heads),
+        out_shape=shapes,
+        in_specs=[vmem, vmem, vmem, smem] + [vmem] * 5 + [hbm, hbm, hbm],
+        out_specs=(vmem, vmem),
+        scratch_shapes=[
+            pltpu.VMEM((model, ff), bf16),
+            pltpu.VMEM((model, ff), bf16),
+            pltpu.VMEM((ff, model), bf16),
+            pltpu.VMEM((n, rows, QKD), bf16),
+            pltpu.VMEM((n, rows, QKD), bf16),
+            pltpu.VMEM((2, n, rows, VD // 2), bf16),
+            pltpu.VMEM((n, rows, VD), bf16),
+            pltpu.VMEM((n // 2, rows, VD), bf16),
+            pltpu.VMEM((n // 2, rows, VD), bf16),
+            pltpu.VMEM((heads, rows, VD), bf16),
+            pltpu.VMEM((TOP, rows_b, n * slots), bf16),
+            pltpu.VMEM((n, slots, width), bf16),
+            pltpu.VMEM((4, n, slots, width), bf16),
+            pltpu.VMEM((4, n, slots, width), bf16),
+            pltpu.VMEM((2, n, slots, width), bf16),
+            pltpu.VMEM((n, slots, width), bf16),
+            pltpu.VMEM((n, slots, width), bf16),
+            pltpu.VMEM((n, slots, width), bf16),
+            pltpu.VMEM((n, slots, width), bf16),
+            dma((3,)),
+            dma((n,)),
+            dma((n,)),
+            dma((n,)),
+            dma((n,)),
+            dma((2, n)),
+            dma((2, n)),
+            dma((3, n)),
+            dma((3, n)),
+            dma((n,)),
+            dma((n,)),
+            dma((n // 2,)),
+            dma((n // 2,)),
+            dma((n // 2,)),
+            dma((n // 2,)),
+            dma((2,)),
+            dma((2,)),
+            dma((n,)),
+            dma((n,)),
+            dma((n,)),
+            dma((n,)),
+        ],
+        compiler_params=pltpu.CompilerParams(
+            collective_id=0, has_side_effects=True, vmem_limit_bytes=56 * 1024 * 1024
+        ),
+    )(
+        queries,
+        key_rows,
+        values,
+        lambdas,
+        head_gain[None, :],
+        tokens,
+        moe_gain[None, :],
+        routes,
+        route_scores,
+        w_gate,
+        w_up,
+        w_down,
+    )
     return tuple(
         pl.pallas_call(
-            functools.partial(step_kernel, n, heads),
-            out_shape=(
-                jax.ShapeDtypeStruct(queries.shape, bf16),
-                jax.ShapeDtypeStruct((rows_b, width), bf16),
-            ),
-            in_specs=[vmem, vmem, vmem, smem, vmem, vmem, vmem, vmem, hbm, hbm, hbm],
-            out_specs=(vmem, vmem),
-            scratch_shapes=[
-                pltpu.VMEM((model, ff), bf16),
-                pltpu.VMEM((model, ff), bf16),
-                pltpu.VMEM((ff, model), bf16),
-                pltpu.VMEM((n, rows, QKD), bf16),
-                pltpu.VMEM((n, rows, QKD), bf16),
-                pltpu.VMEM((n, rows, VD), bf16),
-                pltpu.VMEM((n, rows, VD), bf16),
-                pltpu.VMEM((n, rows, VD), bf16),
-                pltpu.VMEM((4, n, slots, width), bf16),
-                pltpu.VMEM((4, n, slots, width), bf16),
-                pltpu.VMEM((2, n, slots, width), bf16),
-                pltpu.VMEM((n, slots, width), bf16),
-                pltpu.VMEM((n, slots, width), bf16),
-                pltpu.VMEM((n, slots, width), bf16),
-                pltpu.VMEM((n, slots, width), bf16),
-                dma((3,)),
-                dma((n,)),
-                dma((n,)),
-                dma((n,)),
-                dma((n,)),
-                dma((2, n)),
-                dma((2, n)),
-                dma((3, n)),
-                dma((3, n)),
-                dma((n,)),
-                dma((n,)),
-                dma((2,)),
-                dma((2,)),
-                dma((n,)),
-                dma((n,)),
-                dma((n,)),
-                dma((n,)),
-            ],
-            compiler_params=pltpu.CompilerParams(
-                collective_id=0, has_side_effects=True, vmem_limit_bytes=56 * 1024 * 1024
-            ),
-        )(
-            queries,
-            key_rows,
-            values,
-            lambdas,
-            head_gain[None, :],
-            outgoing,
-            pick,
-            gate_weights,
-            w_gate,
-            w_up,
-            w_down,
-        )
+            hand_over, out_shape=shapes, in_specs=[vmem, vmem], out_specs=(vmem, vmem)
+        )(*held)
     )
 
 

time: 80.2 us -> 66.7 us (0.83); the launches traced: 78.6 us -> 66.5 us
  other arithmetic: 5.44 us -> 0 us
  Pallas kernels: 66.2 us -> 63.1 us
  local copies, waits for them, and re-layouts: 5.14 us -> 2.76 us
  matrix products: 1.15 us -> 0 us
    pallas_call x1 -> x2, Pallas kernels: 66.2 us -> 63.1 us  [the longest x1 61.4 us: local(): pl.pallas_call(functools.partial(step_kernel, n, heads), out_shape=shapes...]
    reduce_sum x3 -> x0, other arithmetic: 2.12 us -> none  [the longest x1 1.25 us: local(): jnp.mean(token_f32 * token_f32, axis=-1, keepdims=True) + moe_eps]
    unnamed x5 -> x2, local copies, waits for them, and re-layouts: 4.01 us -> 2.76 us
    convert_element_type x2 -> x0, other arithmetic: 1.22 us -> none  [the longest x1 1.14 us: local(): token_f32 = tokens.astype(jnp.float32)]
    dot_general x1 -> x0, matrix products: 1.15 us -> none  [local(): lax.dot_general(pick[0] + pick[1], mine, (((0,), (0,)), ((), ())), prefer...]
where the time goes in v2:
time: 66.7 us; the launch traced here: 66.5 us
  Pallas kernels  63.1 us (95%)
  local copies, waits for them, and re-layouts  2.76 us (4%)
    pallas_call x1, Pallas kernels, local(): pl.pallas_call(functools.partial(step_kernel, n, heads), out_shape=shapes...  61.4 us
    unnamed x2, local copies, waits for them, and re-layouts  2.76 us
    pallas_call x1, Pallas kernels, local(): pl.pallas_call(hand_over, out_shape=shapes, in_specs=[vmem, vmem], out_sp...  1.74 us

profile of v2, /device:TPU:24, one launch (start us, length us, event | category | flops | bytes accessed | tf_op | source)
XLA Modules:
  0.0 66.5 jit_solution(7863392739110883287)
XLA Ops:
  0.6 1.4 %copy.14.routes_ref = s32[64,2]{1,0:T(8,128)} copy(s32[64,2]{0,1:T(2,128)} %param.19) | data formatting | bytes 1024 | tf_op args[7]
  2.0 1.4 %copy.15.score_ref = f32[64,2]{1,0:T(8,128)} copy(f32[64,2]{0,1:T(2,128)} %param.20) | data formatting | bytes 1024 | tf_op args[8]
  3.4 61.4 %shard_map.131 = (bf16[128,1024]{1,0:T(8,128)(2,1)}, bf16[64,1024]{1,0:T(8,128)(2,1)}) custom-call(bf16[128,1024]{1,0:T(8,128)(2,1)} %q_ref.1, bf16[128,1024]{1,0:T(8,128)(2,1)} %k_ref.1, bf16[128,1024]{1,0:T(8,128)(2,1)} %v_ref.1, f32[4]{0:T(128)} %lam_ref.1, f32[1,256]{1,0:T(1,128)} %bitcast.3, bf16[64,4096]{1,0:T(8,128)(2,1)} %tokens_ref.1, ...), custom_call_target="tpu_custom_call" | custom-call | tf_op jit(solution)/shard_map/pallas_call | solution.py:542
  64.8 1.7 %shard_map.132 = (bf16[128,1024]{1,0:T(8,128)(2,1)}, bf16[64,1024]{1,0:T(8,128)(2,1)}) custom-call(bf16[128,1024]{1,0:T(8,128)(2,1)} %get-tuple-element.4.att_ref, bf16[64,1024]{1,0:T(8,128)(2,1)} %get-tuple-element.5.out_ref), custom_call_target="tpu_custom_call" | custom-call | tf_op jit(solution)/shard_map/pallas_call | solution.py:607

commit v3 on v2

--- a/solution.py
+++ b/solution.py
@@ -271,20 +271,26 @@
         tokens_ref[:, features].astype(jnp.float32) * inverse * moe_gain_ref[:, features]
     ).astype(jnp.bfloat16)
     lane = lax.broadcasted_iota(jnp.int32, (rows_b, 128), 1)
-    named = [routes_ref[:, c : c + 1] == lane for c in range(TOP)]
+    square = (rows_b, rows_b)
+    row_at = lax.broadcasted_iota(jnp.int32, square, 0)
+    column_at = lax.broadcasted_iota(jnp.int32, square, 1)
+
+    def upright(ref, c):
+        line = jnp.broadcast_to(ref[c : c + 1, :], square)
+        return jnp.sum(
+            jnp.where(row_at == column_at, line, jnp.zeros_like(line)), axis=1, keepdims=True
+        )
+
+    named_by = [upright(routes_ref, c) for c in range(TOP)]
+    named = [named_by[c] == lane for c in range(TOP)]
     either = jnp.where(named[0] | named[1], 1.0, 0.0).astype(jnp.bfloat16)
-    square = (rows_b, rows_b)
-    below = jnp.where(
-        lax.broadcasted_iota(jnp.int32, square, 1) < lax.broadcasted_iota(jnp.int32, square, 0),
-        1.0,
-        0.0,
-    ).astype(jnp.bfloat16)
+    below = jnp.where(column_at < row_at, 1.0, 0.0).astype(jnp.bfloat16)
     before = jnp.dot(below, either, preferred_element_type=jnp.float32)
     slot_ids = lax.broadcasted_iota(jnp.int32, (rows_b, total), 1).astype(jnp.float32)
     chosen = jnp.zeros((rows_b, total), jnp.float32)
     for c in range(TOP):
         position = jnp.sum(jnp.where(named[c], before, 0.0), axis=1, keepdims=True)
-        slot = routes_ref[:, c : c + 1].astype(jnp.float32) * slots + position
+        slot = named_by[c].astype(jnp.float32) * slots + position
         hit = jnp.where(slot == slot_ids, 1.0, 0.0)
         pick[c] = hit.astype(jnp.bfloat16)
         chosen = chosen + hit
@@ -365,6 +371,12 @@
     more = first_products(tp_both)
     gate, up = gate + more[0], up + more[1]
     sent += tok_copies + y_copies + core_copies[0] + core_copies[1]
+    for j in range(1, n):
+        s = source(j)
+        unit_copies[0, j].wait_recv()
+        c = remote(vbuf.at[side, s], vbuf.at[side, s], v_send.at[s], v_recv.at[s], pair, tp)
+        c.start()
+        v_copies.append(c)
     hidden = (jax.nn.silu(gate) * up).astype(jnp.bfloat16)
 
     loads[2].wait()
@@ -395,12 +407,6 @@
     sent += near_copies + far_copies
     near_copies[1].wait_recv()
 
-    for j in range(1, n):
-        s = source(j)
-        unit_copies[0, j].wait_recv()
-        c = remote(vbuf.at[side, s], vbuf.at[side, s], v_send.at[s], v_recv.at[s], pair, tp)
-        c.start()
-        v_copies.append(c)
     for j in range(1, n):
         unit_copies[1, j].wait_recv()
         unit_copies[2, j].wait_recv()
@@ -491,7 +497,7 @@
 
     for c in back_copies:
         c.wait_recv()
-    first, second = score_ref[:, 0:1], score_ref[:, 1:2]
+    first, second = upright(score_ref, 0), upright(score_ref, 1)
     top = jnp.maximum(first, second)
     raised = (jnp.exp(first - top), jnp.exp(second - top))
     returned = ret[...].reshape(total, width)
@@ -597,8 +603,8 @@
         head_gain[None, :],
         tokens,
         moe_gain[None, :],
-        routes,
-        route_scores,
+        routes.T,
+        route_scores.T,
         w_gate,
         w_up,
         w_down,

time: 66.7 us -> 63.7 us (0.955)
  local copies, waits for them, and re-layouts: 2.76 us -> 0 us
    unnamed x2 -> x0, local copies, waits for them, and re-layouts: 2.76 us -> none
where the time goes in v3:
time: 63.7 us; the launch traced here: 63.3 us
  Pallas kernels  62.6 us (98%)
  between operations  0.64 us (1%)
    pallas_call x1, Pallas kernels, local(): pl.pallas_call(functools.partial(step_kernel, n, heads), out_shape=shapes...  60.9 us
    pallas_call x1, Pallas kernels, local(): pl.pallas_call(hand_over, out_shape=shapes, in_specs=[vmem, vmem], out_sp...  1.74 us

profile of v3, /device:TPU:24, one launch (start us, length us, event | category | flops | bytes accessed | tf_op | source)
XLA Modules:
  0.0 63.3 jit_solution(9924183119953096533)
XLA Ops:
  0.6 60.9 %shard_map.131 = (bf16[128,1024]{1,0:T(8,128)(2,1)}, bf16[64,1024]{1,0:T(8,128)(2,1)}) custom-call(bf16[128,1024]{1,0:T(8,128)(2,1)} %q_ref.1, bf16[128,1024]{1,0:T(8,128)(2,1)} %k_ref.1, bf16[128,1024]{1,0:T(8,128)(2,1)} %v_ref.1, f32[4]{0:T(128)} %lam_ref.1, f32[1,256]{1,0:T(1,128)} %bitcast.5, bf16[64,4096]{1,0:T(8,128)(2,1)} %tokens_ref.1, ...), custom_call_target="tpu_custom_call" | custom-call | tf_op jit(solution)/shard_map/pallas_call | solution.py:548
  61.5 1.7 %shard_map.132 = (bf16[128,1024]{1,0:T(8,128)(2,1)}, bf16[64,1024]{1,0:T(8,128)(2,1)}) custom-call(bf16[128,1024]{1,0:T(8,128)(2,1)} %get-tuple-element.4.att_ref, bf16[64,1024]{1,0:T(8,128)(2,1)} %get-tuple-element.5.out_ref), custom_call_target="tpu_custom_call" | custom-call | tf_op jit(solution)/shard_map/pallas_call | solution.py:613
